TPU v7x, 32 devices: a whole 2x2x4 slice. The times are simulated.
32 devices in a mesh: sp: 8 (over z, y), tp: 4 (over x, core).
Axes of the slice: x: 2, y: 2, z: 4, core: 2. Of those that a mesh axis runs over, the one named last changes fastest.
Arguments:
- layer_input: bfloat16 [8, 1024, 2048], P(None, ('sp', 'tp')), may hold values from -6 to 6
- input_gain: float32 [2048], replicated, may hold values from 0.5 to 1.5
- narrowing_matrix: bfloat16 [2048, 512], replicated, may hold values from -0.125 to 0.125
- rotary_down: bfloat16 [2048, 64], replicated, may hold values from -0.125 to 0.125
- summary_scaling: float32 [512], replicated, may hold values from 0.5 to 1.5
- lookup_widening: bfloat16 [512, 16, 128], P('tp'), may hold values from -0.25 to 0.25
- payload_widening: bfloat16 [512, 16, 128], P('tp'), may hold values from -0.25 to 0.25
- query_nope: bfloat16 [8, 16, 128], P('sp', 'tp'), may hold values from -6 to 6
- query_rotary: bfloat16 [8, 16, 64], P('sp', 'tp'), may hold values from -6 to 6
Outputs:
- stored_summaries: bfloat16 [8, 1024, 512], P('sp', None, 'tp')
- rotary_cache: bfloat16 [8, 1024, 64], P('sp', None, 'tp')
- first_read: bfloat16 [8, 16, 128], P('sp', 'tp')
All inputs are finite; a program needn't handle non-finite values.
Results may differ from a plain program's by a relative error of at most 0.02.
Values may be sent and summed in bfloat16 or wider, within the bound.
A program may use at most 64 MiB of HBM per device.

v0:
```python
import jax
import jax.numpy as jnp
from jax import lax
from jax.sharding import PartitionSpec as P

QK_ROPE = 64
PLAIN_MATCH_SPAN = 128


norm_eps = 1e-06
rotary_base = 10000.0


def summed_rows(portion, width, axis):
    count = width * lax.axis_size(axis)
    return lax.psum_scatter(portion(jnp.int32(0), count), axis, scatter_dimension=0, tiled=True)


def rescaled_lines(vector):
    return vector * lax.rsqrt(jnp.mean(vector * vector, axis=-1, keepdims=True) + norm_eps)


def rotate(vector, position):
    half_width = vector.shape[-1] // 2
    frequency = 1.0 / rotary_base ** (
        jnp.arange(half_width, dtype=jnp.float32) * 2.0 / vector.shape[-1]
    )
    angles = position * frequency
    first_half = vector[..., :half_width]
    second_half = vector[..., half_width:]
    return jnp.concatenate(
        [
            first_half * jnp.cos(angles) - second_half * jnp.sin(angles),
            second_half * jnp.cos(angles) + first_half * jnp.sin(angles),
        ],
        axis=-1,
    )


def to_pieces(array, sp_count, tp_count):
    seq_count, pos_local, cache_width = array.shape
    seq_each = seq_count // sp_count
    width_each = cache_width // tp_count
    array = array.reshape(sp_count, seq_each, pos_local, tp_count, width_each)
    array = array.transpose(0, 3, 1, 2, 4)
    return array.reshape(sp_count * tp_count, seq_each, pos_local, width_each)


def shards(
    layer_input,
    input_gain,
    narrowing_matrix,
    rotary_down,
    summary_scaling,
    lookup_widening,
    payload_widening,
    query_nope,
    query_rotary,
):
    seq_count, pos_local, feature_width = layer_input.shape
    sp_count = lax.axis_size("sp")
    tp_count = lax.axis_size("tp")
    block_index = lax.axis_index(("sp", "tp"))
    normed = (rescaled_lines(layer_input.astype(jnp.float32)) * input_gain).astype(jnp.bfloat16)
    flat_rows = normed.reshape(seq_count * pos_local, feature_width)
    hidden_summary = jnp.dot(
        flat_rows, narrowing_matrix, preferred_element_type=jnp.float32
    ).astype(jnp.bfloat16)
    rotary = jnp.dot(flat_rows, rotary_down, preferred_element_type=jnp.float32).astype(
        jnp.bfloat16
    )
    hidden_summary = (
        (rescaled_lines(hidden_summary.astype(jnp.float32)) * summary_scaling)
        .astype(jnp.bfloat16)
        .reshape(seq_count, pos_local, -1)
    )
    positions = (block_index * pos_local + jnp.arange(pos_local, dtype=jnp.int32)).astype(
        jnp.float32
    )[None, :, None]
    rotary = rotate(rotary.astype(jnp.float32).reshape(seq_count, pos_local, -1), positions).astype(
        jnp.bfloat16
    )
    moved = (
        lax.all_to_all(
            to_pieces(hidden_summary, sp_count, tp_count),
            ("sp", "tp"),
            split_axis=0,
            concat_axis=2,
            tiled=True,
        ),
        lax.all_to_all(
            to_pieces(rotary, sp_count, tp_count),
            ("sp", "tp"),
            split_axis=0,
            concat_axis=2,
            tiled=True,
        ),
    )
    hidden_summary = moved[0][0]
    rotary = moved[1][0]
    pos_total = hidden_summary.shape[1]
    rot_each = rotary.shape[2]
    head_each = query_nope.shape[1]
    query_all, turn_all = (
        lax.all_gather(query_nope, "tp", axis=1, tiled=True),
        lax.all_gather(query_rotary, "tp", axis=1, tiled=True),
    )
    absorbed = jnp.einsum(
        "shd,chd->shc", query_all, lookup_widening, preferred_element_type=jnp.float32
    ).astype(jnp.bfloat16)
    query_turned = rotate(turn_all.astype(jnp.float32), jnp.float32(pos_total)).astype(jnp.bfloat16)
    turned_mine = lax.dynamic_slice_in_dim(
        query_turned, lax.axis_index("tp") * rot_each, rot_each, 2
    )
    score_scale = (PLAIN_MATCH_SPAN + QK_ROPE) ** (-0.5)
    partial_value = (
        jnp.einsum("shc,spc->shp", absorbed, hidden_summary, preferred_element_type=jnp.float32)
        + jnp.einsum("shr,spr->shp", turned_mine, rotary, preferred_element_type=jnp.float32)
    ) * score_scale
    scores = lax.psum(partial_value.astype(jnp.bfloat16), "tp").astype(jnp.float32)
    attention = jax.nn.softmax(scores, axis=-1).astype(jnp.bfloat16)
    context = jnp.einsum(
        "shp,spc->shc", attention, hidden_summary, preferred_element_type=jnp.float32
    ).astype(jnp.bfloat16)

    def project_heads(row_start, row_count):
        part_context = lax.dynamic_slice_in_dim(context, row_start, row_count, 1)
        part_weight = lax.dynamic_slice_in_dim(payload_widening, row_start, row_count, 1)
        return jnp.einsum(
            "shc,chv->hsv", part_context, part_weight, preferred_element_type=jnp.float32
        )

    values = summed_rows(project_heads, head_each, "tp")
    first_read = rescaled_lines(values.transpose(1, 0, 2)).astype(jnp.bfloat16)
    return (hidden_summary, rotary, first_read)


def solution(mesh):
    return jax.shard_map(
        shards,
        mesh=mesh,
        in_specs=(
            P(None, ("sp", "tp"), None),
            P(),
            P(),
            P(),
            P(),
            P("tp", None, None),
            P("tp", None, None),
            P("sp", "tp", None),
            P("sp", "tp", None),
        ),
        out_specs=(P("sp", None, "tp"), P("sp", None, "tp"), P("sp", "tp", None)),
        check_vma=False,
    )
```

profile of v0, /device:TPU:0, one launch (start us, length us, event | category | flops | bytes accessed | tf_op | source)
XLA Modules:
  0.0 55.6 jit_solution(11520406021461989264)
XLA Ops:
  0.6 0.0 copy-start
  0.6 0.0 copy-start.1
  0.7 1.7 %fusion = f32[8,32]{1,0:T(8,128)S(1)} fusion(bf16[8,32,2048]{2,1,0:T(8,128)(2,1)} %param.9), kind=kLoop, calls=%fused_computation.2 | loop fusion | flops 1572608 | bytes 1049600 | tf_op jit(solution)/shard_map/reduce_sum | solution.py:20
  2.4 0.0 copy-start.3
  2.4 1.5 %fusion.2 = bf16[8,32,2048]{2,1,0:T(8,128)(2,1)S(1)} fusion(bf16[8,32,2048]{2,1,0:T(8,128)(2,1)} %param.9, f32[2048]{0:T(1024)} %param.10, f32[8,32]{1,0:T(8,128)S(1)} %add_rsqrt_fusion), kind=kLoop, calls=%fused_computation.4 | loop fusion | flops 2097152 | bytes 2106368 | tf_op jit(solution)/shard_map/convert_element_type | solution.py:64
  3.9 0.0 copy-done.1
  4.0 0.4 fusion.6
  4.4 0.1 copy.33
  4.5 0.1 multiply_cosine_fusion
  4.6 0.1 subtract_convert_fusion
  4.8 0.1 pad_maximum_fusion
  4.9 0.1 copy.34
  5.0 0.0 copy-start.2
  5.0 0.8 %reshape.300 = bf16[32,2,256]{2,1,0:T(2,128)(2,1)} reshape(bf16[32,1,16,32]{3,2,1,0:T(8,128)(2,1)S(1)} %bitcast.62) | data formatting | bytes 65536
  5.8 7.4 %all-to-all-start.1 = ((bf16[32,2,256]{2,1,0:T(2,128)(2,1)}), bf16[32,2,256]{2,1,0:T(2,128)(2,1)S(1)}, u32[]{:S(2)}, u32[]{:S(2)}) async-start(bf16[32,2,256]{2,1,0:T(2,128)(2,1)} %reshape.300), calls=%async_computation.1 | async-start | bytes 65536 | tf_op jit(solution)/shard_map/all_to_all | solution.py:91
  13.1 0.0 copy-done.3
  13.2 5.2 %all_gather.7 = bf16[1,16,64]{2,0,1:T(2,128)(2,1)S(1)} all-gather(bf16[1,4,64]{2,0,1:T(2,128)(2,1)S(1)} %copy.37), channel_id=1, replica_groups=mesh['sp'=8,'tp'=4] {'tp'}, dimensions={1}, use_global_device_ids=true | all-gather | bytes 2560 | tf_op jit(solution)/shard_map/all_gather | solution.py:106
  18.4 0.0 copy-done
  18.4 0.8 %multiply_reduce_fusion = (f32[256]{0:T(256)S(1)}, f32[256,512]{1,0:T(8,128)S(1)}) fusion(bf16[256,2048]{1,0:T(8,128)(2,1)S(1)} %bitcast.57, bf16[2048,512]{1,0:T(8,128)(2,1)S(1)} %copy-done), kind=kOutput, calls=%fused_computation.20 | convolution fusion | flops 537394944 | bytes 3671040 | tf_op jit(solution)/shard_map/dot_general | solution.py:66
  19.2 0.0 copy-start.4
  19.2 0.0 copy-start.7
  19.2 0.0 copy-start.5
  19.2 0.0 copy-done.2
  19.2 0.1 multiply_convert_fusion
  19.4 0.1 reshape_reshape.3
  19.4 0.0 copy-start.6
  19.4 0.8 %copy.31 = bf16[8,1,32,4,128]{4,2,3,0,1:T(8,128)(2,1)} copy(bf16[8,1,32,4,128]{4,3,2,0,1:T(4,128)(2,1)S(1)} %reshape_reshape.3) | data formatting | bytes 524288 | tf_op jit(solution)/shard_map/reshape;reshape | solution.py:44
  20.2 0.2 all-to-all-done.1
  20.4 5.5 %all-to-all-start = ((bf16[32,1,32,128]{3,2,1,0:T(8,128)(2,1)}), bf16[32,1,32,128]{3,2,1,0:T(8,128)(2,1)S(1)}, u32[]{:S(2)}, u32[]{:S(2)}) async-start(bf16[32,1,32,128]{3,2,1,0:T(8,128)(2,1)} %bitcast.3), calls=%async_computation | async-start | bytes 524288 | tf_op jit(solution)/shard_map/all_to_all | solution.py:84
  26.1 0.0 copy-done.4
  26.1 0.0 copy-done.7
  26.1 0.6 %dynamic-slice = u32[1]{0:T(128)} dynamic-slice(u32[32]{0:T(128)S(1)} %copy-done.7, u32[]{:T(128)S(6)} %add.73), dynamic_slice_sizes={1} | dynamic-slice | bytes 12
  27.3 5.2 %all_gather.6 = bf16[1,16,128]{2,0,1:T(2,128)(2,1)S(1)} all-gather(bf16[1,4,128]{2,0,1:T(2,128)(2,1)S(1)} %copy.36), channel_id=1, replica_groups=mesh['sp'=8,'tp'=4] {'tp'}, dimensions={1}, use_global_device_ids=true | all-gather | bytes 5120 | tf_op jit(solution)/shard_map/all_gather | solution.py:105
  32.5 0.1 subtract_convert_fusion.1
  32.6 0.0 copy-done.5
  32.6 0.4 fusion.11
  33.0 0.2 reshape.301
  33.2 0.2 reshape.287
  33.3 0.8 %squeeze.7 = bf16[1,1024,16]{1,2,0:T(8,128)(2,1)} reshape(bf16[32,1,32,16]{2,0,3,1:T(8,128)(2,1)S(1)} %copy.35) | data formatting | bytes 65536 | tf_op jit(solution)/shard_map/squeeze | solution.py:100
  34.1 2.4 %all-to-all-done = bf16[32,1,32,128]{3,2,1,0:T(8,128)(2,1)S(1)} async-done(((bf16[32,1,32,128]{3,2,1,0:T(8,128)(2,1)}), bf16[32,1,32,128]{3,2,1,0:T(8,128)(2,1)S(1)}, u32[]{:S(2)}, u32[]{:S(2)}) %all-to-all-start) | async-done | bytes 262176 | tf_op jit(solution)/shard_map/all_to_all | solution.py:84
  36.5 0.2 fusion.25
  36.7 0.2 fusion.7
  36.9 10.6 %psum.7 = bf16[1,16,1024]{2,1,0:T(8,128)(2,1)S(1)} all-reduce(bf16[1,16,1024]{2,1,0:T(8,128)(2,1)S(1)} %fusion.7), channel_id=1, replica_groups=mesh['sp'=8,'tp'=4] {'tp'}, use_global_device_ids=true, to_apply=%region_2.0 | all-reduce | flops 16384 | bytes 65536 | tf_op jit(solution)/shard_map/psum | solution.py:120
  47.5 0.1 reduce_max.14
  47.6 0.2 fusion.13
  47.8 0.2 fusion.8
  48.1 0.0 copy-done.6
  48.1 0.3 fusion.9
  48.3 5.8 %all-reduce = f32[16,1,128]{2,0,1:T(8,128)S(1)} all-reduce(f32[16,1,128]{2,0,1:T(8,128)S(1)} %bitcast.64), channel_id=2, replica_groups=mesh['sp'=8,'tp'=4] {'tp'}, use_global_device_ids=true, to_apply=%region_5.0.clone | all-reduce | flops 2048 | bytes 16384
  54.1 0.1 multiply_reduce_fusion.1
  54.2 0.6 %multiply_convert_fusion.1 = bf16[1,4,128]{2,1,0:T(4,128)(2,1)} fusion(f32[16,1,128]{2,0,1:T(8,128)S(1)} %all-reduce, u32[]{:T(128)S(6)} %multiply.33, f32[4]{0:T(128)S(1)} %add_rsqrt_fusion.2), kind=kLoop, calls=%fused_computation.46 | loop fusion | flops 1024 | bytes 3092 | tf_op jit(solution)/shard_map/convert_element_type | solution.py:134
  54.9 0.7 %copy.56 = bf16[1,1024,128]{2,1,0:T(8,128)(2,1)} copy(bf16[1,1024,128]{2,1,0:T(8,128)(2,1)S(1)} %bitcast.60) | data formatting | bytes 524288
  (11 shorter events, 0.1 us)
Async XLA Ops:
  0.6 17.8 %copy-start = (bf16[2048,512]{1,0:T(8,128)(2,1)S(1)}, bf16[2048,512]{1,0:T(8,128)(2,1)}, u32[]{:S(2)}) copy-start(bf16[2048,512]{1,0:T(8,128)(2,1)} %param.11) | copy-start | bytes 6291460
  0.6 3.3 %copy-start.1 = (bf16[2048,64]{0,1:T(8,128)(2,1)S(1)}, bf16[2048,64]{0,1:T(8,128)(2,1)}, u32[]{:S(2)}) copy-start(bf16[2048,64]{0,1:T(8,128)(2,1)} %param.12) | copy-start | bytes 786436
  2.4 10.8 %copy-start.3 = (bf16[1,4,64]{2,1,0:T(4,128)(2,1)S(1)}, bf16[1,4,64]{2,1,0:T(4,128)(2,1)}, u32[]{:S(2)}) copy-start(bf16[1,4,64]{2,1,0:T(4,128)(2,1)} %param.17) | copy-start | bytes 1540
  5.0 14.2 %copy-start.2 = (f32[512]{0:T(512)S(1)}, f32[512]{0:T(512)}, u32[]{:S(2)}) copy-start(f32[512]{0:T(512)} %param.13) | copy-start | bytes 6148
  5.8 14.7 %all-to-all-start.1 = ((bf16[32,2,256]{2,1,0:T(2,128)(2,1)}), bf16[32,2,256]{2,1,0:T(2,128)(2,1)S(1)}, u32[]{:S(2)}, u32[]{:S(2)}) async-start(bf16[32,2,256]{2,1,0:T(2,128)(2,1)} %reshape.300), calls=%async_computation.1 | async-start | bytes 65536 | tf_op jit(solution)/shard_map/all_to_all | solution.py:91
  19.2 6.9 %copy-start.4 = (bf16[1,4,128]{2,1,0:T(4,128)(2,1)S(1)}, bf16[1,4,128]{2,1,0:T(4,128)(2,1)}, u32[]{:S(2)}) copy-start(bf16[1,4,128]{2,1,0:T(4,128)(2,1)} %param.16) | copy-start | bytes 3076
  19.2 6.9 %copy-start.7 = (u32[32]{0:T(128)S(1)}, u32[32]{0:T(128)}, u32[]{:S(2)}) copy-start(u32[32]{0:T(128)} %constant.54) | copy-start | bytes 388
  19.2 13.4 %copy-start.5 = (bf16[128,16,128]{2,1,0:T(8,128)(2,1)S(1)}, bf16[128,16,128]{2,1,0:T(8,128)(2,1)}, u32[]{:S(2)}) copy-start(bf16[128,16,128]{2,1,0:T(8,128)(2,1)} %param.14) | copy-start | bytes 1572868
  19.4 28.6 %copy-start.6 = (bf16[128,16,128]{2,1,0:T(8,128)(2,1)S(1)}, bf16[128,16,128]{2,1,0:T(8,128)(2,1)}, u32[]{:S(2)}) copy-start(bf16[128,16,128]{2,1,0:T(8,128)(2,1)} %param.15) | copy-start | bytes 1572868
  20.4 16.1 %all-to-all-start = ((bf16[32,1,32,128]{3,2,1,0:T(8,128)(2,1)}), bf16[32,1,32,128]{3,2,1,0:T(8,128)(2,1)S(1)}, u32[]{:S(2)}, u32[]{:S(2)}) async-start(bf16[32,1,32,128]{3,2,1,0:T(8,128)(2,1)} %bitcast.3), calls=%async_computation | async-start | bytes 524288 | tf_op jit(solution)/shard_map/all_to_all | solution.py:84
where the time goes:
time: 55.9 us; the launch traced here: 55.6 us
  blocking collectives  26.8 us (48%)
  starting transfers between devices  12.9 us (23%)
  other arithmetic  4.95 us (9%)
  local copies, waits for them, and re-layouts  4.3 us (8%)
  waiting for transfers between devices  2.64 us (5%)
  matrix products  2.46 us (4%)
  between operations  1.56 us (3%)
    psum x1, blocking collectives, shards(): lax.psum(partial_value.astype(jnp.bfloat16), 'tp').astype(jnp.float32)  10.6 us
    all_to_all x1, starting transfers between devices, shards(): lax.all_to_all(to_pieces(rotary, sp_count, tp_count), ('sp', 'tp'), split...  7.36 us
    unnamed x1, blocking collectives  5.76 us
    all_to_all x1, starting transfers between devices, shards(): lax.all_to_all(to_pieces(hidden_summary, sp_count, tp_count), ('sp', 'tp'...  5.54 us
    all_gather x1, blocking collectives, shards(): lax.all_gather(query_rotary, 'tp', axis=1, tiled=True)  5.23 us
    all_gather x1, blocking collectives, shards(): lax.all_gather(query_nope, 'tp', axis=1, tiled=True)  5.19 us
    all_to_all x1, waiting for transfers between devices, shards(): lax.all_to_all(to_pieces(hidden_summary, sp_count, tp_count), ('sp', 'tp'...  2.4 us
    unnamed x22, local copies, waits for them, and re-layouts  2.26 us
  transfers between devices with their start and end apart: 2, of which 2 were waited for; matrix products, arithmetic and copies ran while one was open for 7% of the time, Pallas kernels for 0%

commit v1 on v0

v1 whole, which is shorter than its diff:
```python
import functools

import jax
import jax.numpy as jnp
from jax import lax
from jax.experimental import pallas as pl
from jax.experimental.pallas import tpu as pltpu
from jax.sharding import PartitionSpec as P

QK_ROPE = 64
PLAIN_MATCH_SPAN = 128

norm_eps = 1e-06
rotary_base = 10000.0
LANES = 128
ROW_CHUNKS = 2
K_CHUNKS = 4
MESH = pl.DeviceIdType.MESH
f32 = jnp.float32
bf16 = jnp.bfloat16


def rescaled_lines(vector):
    return vector * lax.rsqrt(jnp.mean(vector * vector, axis=-1, keepdims=True) + norm_eps)


def iota(shape, axis):
    return lax.broadcasted_iota(jnp.int32, shape, axis)


def one_hot(cond):
    return jnp.where(cond, 1.0, 0.0).astype(bf16)


def dot(a, b):
    return jnp.dot(a, b, preferred_element_type=f32)


def dot_t(a, b):
    return lax.dot_general(a, b, (((1,), (1,)), ((), ())), preferred_element_type=f32)


def kernel(
    dims,
    x_hbm,
    w_hbm,
    wr_hbm,
    lw_hbm,
    pw_hbm,
    gain_ref,
    sgain_ref,
    table_ref,
    q_ref,
    qr_ref,
    cache_out,
    rotary_out,
    read_out,
    x_ref,
    w_ref,
    wr_ref,
    lw_ref,
    pw_ref,
    xn_ref,
    stage,
    rstage,
    lat_recv,
    rot_recv,
    q_recv,
    q_all,
    s_recv,
    v_send,
    v_recv,
    spread,
    unpack,
    rot_full,
    load_sem,
    out_sem,
    lat_sem,
    rot_sem,
    q_send_sem,
    q_recv_sem,
    s_send_sem,
    s_recv_sem,
    v_send_sem,
    v_recv_sem,
):
    sp_count, tp_count = dims
    n = sp_count * tp_count
    seq_count, pos_local, features = x_ref.shape
    latent = w_ref.shape[1]
    rope = wr_ref.shape[0]
    width = latent // tp_count
    rot_each = rope // tp_count
    packs = LANES // rot_each
    prow = pos_local // packs
    head_each, plain = q_ref.shape
    heads = head_each * tp_count
    total = n * pos_local
    my_sp = lax.axis_index("sp")
    my_tp = lax.axis_index("tp")
    me = my_sp * tp_count + my_tp

    loads = {}

    def load(key, index, src, dst):
        copy = pltpu.make_async_copy(src, dst, load_sem.at[index])
        copy.start()
        loads[key] = copy

    kdepth = features // K_CHUNKS
    for j in range(seq_count):
        load(("x", j), j, x_hbm.at[lax.rem(my_sp + 1 + j, sp_count)], x_ref.at[j])
    for k in range(K_CHUNKS):
        rows = pl.ds(k * kdepth, kdepth)
        load(("w", k), seq_count + k, w_hbm.at[rows], w_ref.at[rows])
    base = seq_count + K_CHUNKS
    load("wr", base, wr_hbm, wr_ref)
    load("lw", base + 1, lw_hbm, lw_ref)
    load("pw", base + 2, pw_hbm, pw_ref)

    barrier = pltpu.get_barrier_semaphore()

    def greet(i, carry):
        other = lax.rem(me + 1 + i, n)
        pl.semaphore_signal(
            barrier,
            inc=1,
            device_id=(lax.div(other, tp_count), lax.rem(other, tp_count)),
            device_id_type=MESH,
        )
        return carry

    lax.fori_loop(0, n - 1, greet, 0)

    q_recv[my_tp] = jnp.zeros(q_recv.shape[1:], f32)
    q_recv[my_tp, :, :plain] = q_ref[...].astype(f32)
    q_recv[my_tp, :, plain : plain + rope] = qr_ref[...].astype(f32)

    cos = table_ref[0, :pos_local, :]
    sin = table_ref[1, :pos_local, :]
    half = rope // 2
    row_r, col_r = iota((rope, rope), 0), iota((rope, rope), 1)
    swap = (
        jnp.where((row_r == col_r + half), -1.0, 0.0)
        + jnp.where((row_r + half == col_r), 1.0, 0.0)
    ).astype(bf16)
    wide = (rope, tp_count * LANES)
    tile = one_hot(
        iota(wide, 0)
        == iota(wide, 1) // LANES * rot_each + iota(wide, 1) % rot_each
    )

    pairs = []

    def remote(src, dst, send, recv, sp, tp):
        copy = pltpu.make_async_remote_copy(
            src_ref=src,
            dst_ref=dst,
            send_sem=send,
            recv_sem=recv,
            device_id=(sp, tp),
            device_id_type=MESH,
        )
        copy.start()
        return copy

    chunk_seq = seq_count // ROW_CHUNKS
    chunk = chunk_seq * pos_local
    pick_shape = (chunk_seq * prow, chunk)
    pick_row, pick_col = iota(pick_shape, 0), iota(pick_shape, 1)
    pick = one_hot(
        (pick_row // prow == pick_col // pos_local) & (pick_row % prow == pick_col % prow)
    )
    mask_shape = (chunk, tp_count * LANES)
    keep = (iota(mask_shape, 1) % LANES) // rot_each == (
        iota(mask_shape, 0) % pos_local
    ) // prow

    for c in range(ROW_CHUNKS):
        for j in range(chunk_seq):
            at = c * chunk_seq + j
            loads[("x", at)].wait()
            rows = rescaled_lines(x_ref[at].astype(f32)) * gain_ref[...]
            xn_ref[pl.ds(j * pos_local, pos_local), :] = rows.astype(bf16)
        acc = None
        for k in range(K_CHUNKS):
            if c == 0:
                loads[("w", k)].wait()
            part = dot(
                xn_ref[:, k * kdepth : (k + 1) * kdepth],
                w_ref[k * kdepth : (k + 1) * kdepth, :],
            )
            acc = part if acc is None else acc + part
        if c == 0:
            loads["wr"].wait()
        rot = dot_t(xn_ref[...], wr_ref[...]).astype(bf16)
        hidden = rescaled_lines(acc.astype(bf16).astype(f32)) * sgain_ref[...]
        swapped = dot(rot, swap)
        turned = (
            rot.astype(f32).reshape(chunk_seq, pos_local, rope) * cos[None]
            + swapped.reshape(chunk_seq, pos_local, rope) * sin[None]
        ).reshape(chunk, rope)
        copies = dot(turned.astype(bf16), tile)
        packed = dot(pick, jnp.where(keep, copies, 0.0).astype(bf16))
        for j in range(chunk_seq):
            for t in range(tp_count):
                at = (c * chunk_seq + j) * tp_count + t
                stage[at] = hidden[
                    j * pos_local : (j + 1) * pos_local, t * width : (t + 1) * width
                ].astype(bf16)
                rstage[at] = packed[
                    j * prow : (j + 1) * prow, t * LANES : (t + 1) * LANES
                ].astype(bf16)
        if c == 0:
            pl.semaphore_wait(barrier, n - 1)
            for k in range(tp_count - 1):
                peer = lax.rem(my_tp + 1 + k, tp_count)
                pairs.append(
                    remote(
                        q_recv.at[my_tp],
                        q_recv.at[my_tp],
                        q_send_sem.at[k],
                        q_recv_sem.at[k],
                        my_sp,
                        peer,
                    )
                )
        for j in range(chunk_seq):
            order = c * chunk_seq + j
            to_sp = lax.rem(my_sp + 1 + order, sp_count)
            for k in range(tp_count):
                to_tp = lax.rem(my_tp + 1 + k, tp_count)
                at = order * tp_count + to_tp
                if order == seq_count - 1 and k == tp_count - 1:
                    lat_recv[me] = stage[at]
                    rot_recv[me] = rstage[at]
                else:
                    remote(
                        rstage.at[at], rot_recv.at[me], rot_sem.at[0], rot_sem.at[1], to_sp, to_tp
                    )
                    remote(
                        stage.at[at], lat_recv.at[me], lat_sem.at[0], lat_sem.at[1], to_sp, to_tp
                    )

    spread_shape = spread.shape
    spread[...] = one_hot(iota(spread_shape, 0) // heads == iota(spread_shape, 1))
    own_shape = (heads, width * heads)
    own_head = iota(own_shape, 0) == iota(own_shape, 1) % heads
    un_shape = unpack.shape
    un_row, un_col = iota(un_shape, 0), iota(un_shape, 1)
    unpack[...] = one_hot(
        (un_row // pos_local == un_col // prow) & (un_row % prow == un_col % prow)
    )
    rkeep_shape = (total, LANES)
    rkeep = iota(rkeep_shape, 1) // rot_each == (iota(rkeep_shape, 0) % pos_local) // prow
    narrow = (LANES, rot_each)
    fold = one_hot(iota(narrow, 0) % rot_each == iota(narrow, 1))

    for copy in pairs:
        copy.wait()
    for t in range(tp_count):
        q_all[t * head_each : (t + 1) * head_each, :] = q_recv[t]
    queries = q_all[:, :plain].astype(bf16)
    q_rot = q_all[:, plain : plain + rope]
    qcos = table_ref[0, pos_local : pos_local + 1, :]
    qsin = table_ref[1, pos_local : pos_local + 1, :]
    q_turned = (q_rot * qcos + dot(q_rot.astype(bf16), swap) * qsin).astype(bf16)
    share = (rope, rot_each)
    mine = one_hot(iota(share, 0) == iota(share, 1) + my_tp * rot_each)
    q_mine = dot(q_turned, mine).astype(bf16)
    loads["lw"].wait()
    lookup = lw_ref[...].reshape(width * heads, plain)
    every = dot_t(queries, lookup)
    absorbed = dot(jnp.where(own_head, every, 0.0).astype(bf16), spread[...]).astype(bf16)

    pltpu.make_async_copy(
        rot_recv.at[pl.ds(0, n - 1)], rot_recv.at[pl.ds(0, n - 1)], rot_sem.at[1]
    ).wait()
    rot_rows = rot_recv[...].astype(f32).reshape(n * prow, LANES).astype(bf16)
    rot_wide = jnp.where(rkeep, dot(unpack[...], rot_rows), 0.0).astype(bf16)
    rot_cache = dot(rot_wide, fold).astype(bf16)
    rot_full[...] = rot_cache
    rot_store = pltpu.make_async_copy(rot_full, rotary_out, out_sem.at[1])
    rot_store.start()
    rot_part = dot_t(q_mine, rot_cache)

    pltpu.make_async_copy(
        lat_recv.at[pl.ds(0, n - 1)], lat_recv.at[pl.ds(0, n - 1)], lat_sem.at[1]
    ).wait()
    cache_store = pltpu.make_async_copy(lat_recv, cache_out, out_sem.at[0])
    cache_store.start()
    cache = lat_recv[...].reshape(total, width)
    score_scale = (PLAIN_MATCH_SPAN + QK_ROPE) ** (-0.5)
    s_recv[my_tp] = ((dot_t(absorbed, cache) + rot_part) * score_scale).astype(bf16)
    pairs = []
    for k in range(tp_count - 1):
        peer = lax.rem(my_tp + 1 + k, tp_count)
        pairs.append(
            remote(
                s_recv.at[my_tp],
                s_recv.at[my_tp],
                s_send_sem.at[k],
                s_recv_sem.at[k],
                my_sp,
                peer,
            )
        )
    loads["pw"].wait()
    for copy in pairs:
        copy.wait()
    scores = s_recv[0].astype(f32)
    for t in range(1, tp_count):
        scores = scores + s_recv[t].astype(f32)
    top = jnp.max(scores, axis=-1, keepdims=True)
    weights = jnp.exp(scores - top)
    attention = (weights / jnp.sum(weights, axis=-1, keepdims=True)).astype(bf16)
    context = dot(attention, cache).astype(bf16)
    laid = jnp.where(own_head, dot_t(context, spread[...]), 0.0).astype(bf16)
    payload = pw_ref[...].reshape(width * heads, pw_ref.shape[2])
    values = dot(laid, payload)
    for t in range(tp_count):
        v_send[t] = values[t * head_each : (t + 1) * head_each, :]
    v_recv[my_tp] = v_send[my_tp]
    pairs = []
    for k in range(tp_count - 1):
        peer = lax.rem(my_tp + 1 + k, tp_count)
        pairs.append(
            remote(
                v_send.at[peer],
                v_recv.at[my_tp],
                v_send_sem.at[k],
                v_recv_sem.at[k],
                my_sp,
                peer,
            )
        )
    pltpu.make_async_copy(
        rstage.at[pl.ds(0, n - 1)], rstage.at[pl.ds(0, n - 1)], rot_sem.at[0]
    ).wait()
    pltpu.make_async_copy(
        stage.at[pl.ds(0, n - 1)], stage.at[pl.ds(0, n - 1)], lat_sem.at[0]
    ).wait()
    cache_store.wait()
    rot_store.wait()
    for copy in pairs:
        copy.wait()
    summed = v_recv[0]
    for t in range(1, tp_count):
        summed = summed + v_recv[t]
    read_out[...] = rescaled_lines(summed).astype(bf16)


def shards(
    layer_input,
    input_gain,
    narrowing_matrix,
    rotary_down,
    summary_scaling,
    lookup_widening,
    payload_widening,
    query_nope,
    query_rotary,
):
    seq_count, pos_local, features = layer_input.shape
    sp_count = lax.axis_size("sp")
    tp_count = lax.axis_size("tp")
    n = sp_count * tp_count
    assert seq_count == sp_count
    latent = narrowing_matrix.shape[1]
    rope = rotary_down.shape[1]
    width, heads, plain = lookup_widening.shape
    payload = payload_widening.shape[2]
    head_each = query_nope.shape[1]
    rot_each = rope // tp_count
    prow = pos_local * rot_each // LANES
    total = n * pos_local
    block_index = lax.axis_index(("sp", "tp"))
    half = rope // 2
    frequency = 1.0 / rotary_base ** (jnp.arange(half, dtype=f32) * 2.0 / rope)
    frequency = jnp.concatenate([frequency, frequency])
    spots = jnp.arange(pos_local + 8, dtype=jnp.int32)
    spots = jnp.where(spots < pos_local, block_index * pos_local + spots, total)
    angles = spots.astype(f32)[:, None] * frequency[None, :]
    table = jnp.stack([jnp.cos(angles), jnp.sin(angles)])
    any_spec = pl.BlockSpec(memory_space=pl.ANY)
    vmem_spec = pl.BlockSpec(memory_space=pltpu.VMEM)
    dma = pltpu.SemaphoreType.DMA
    cache, rotary, read = pl.pallas_call(
        functools.partial(kernel, (sp_count, tp_count)),
        out_shape=(
            jax.ShapeDtypeStruct((n, pos_local, width), bf16),
            jax.ShapeDtypeStruct((total, rot_each), bf16),
            jax.ShapeDtypeStruct((head_each, payload), bf16),
        ),
        in_specs=[any_spec] * 5 + [vmem_spec] * 5,
        out_specs=(any_spec, any_spec, vmem_spec),
        scratch_shapes=[
            pltpu.VMEM((seq_count, pos_local, features), bf16),
            pltpu.VMEM((features, latent), bf16),
            pltpu.VMEM((rope, features), bf16),
            pltpu.VMEM((width, heads, plain), bf16),
            pltpu.VMEM((width, heads, payload), bf16),
            pltpu.VMEM((seq_count * pos_local // ROW_CHUNKS, features), bf16),
            pltpu.VMEM((n, pos_local, width), bf16),
            pltpu.VMEM((n, prow, LANES), bf16),
            pltpu.VMEM((n, pos_local, width), bf16),
            pltpu.VMEM((n, prow, LANES), bf16),
            pltpu.VMEM((tp_count, head_each, 2 * LANES), f32),
            pltpu.VMEM((heads, 2 * LANES), f32),
            pltpu.VMEM((tp_count, heads, total), bf16),
            pltpu.VMEM((tp_count, head_each, payload), f32),
            pltpu.VMEM((tp_count, head_each, payload), f32),
            pltpu.VMEM((width * heads, width), bf16),
            pltpu.VMEM((total, n * prow), bf16),
            pltpu.VMEM((total, rot_each), bf16),
            dma((seq_count + K_CHUNKS + 3,)),
            dma((2,)),
            dma((2,)),
            dma((2,)),
            dma((tp_count - 1,)),
            dma((tp_count - 1,)),
            dma((tp_count - 1,)),
            dma((tp_count - 1,)),
            dma((tp_count - 1,)),
            dma((tp_count - 1,)),
        ],
        compiler_params=pltpu.CompilerParams(
            collective_id=0, has_side_effects=True, vmem_limit_bytes=63 * 1024 * 1024
        ),
    )(
        layer_input,
        narrowing_matrix,
        rotary_down.T,
        lookup_widening,
        payload_widening,
        input_gain.reshape(1, -1),
        summary_scaling.reshape(1, -1),
        table,
        query_nope[0],
        query_rotary[0],
    )
    return (
        cache.reshape(1, total, width),
        rotary.reshape(1, total, rot_each),
        read.reshape(1, head_each, payload),
    )


def solution(mesh):
    return jax.shard_map(
        shards,
        mesh=mesh,
        in_specs=(
            P(None, ("sp", "tp"), None),
            P(),
            P(),
            P(),
            P(),
            P("tp", None, None),
            P("tp", None, None),
            P("sp", "tp", None),
            P("sp", "tp", None),
        ),
        out_specs=(P("sp", None, "tp"), P("sp", None, "tp"), P("sp", "tp", None)),
        check_vma=False,
    )
```

time: 55.9 us -> 28.7 us (0.51)
  blocking collectives: 26.8 us -> 0 us
  Pallas kernels: 0 us -> 22.3 us
  starting transfers between devices: 12.9 us -> 0 us
  other arithmetic: 4.95 us -> 0.87 us
  waiting for transfers between devices: 2.64 us -> 0 us
  matrix products: 2.46 us -> 0 us
  between operations: 1.56 us -> 0.66 us
    pallas_call x0 -> x1, Pallas kernels: none -> 22.3 us  [shards(): pl.pallas_call(functools.partial(kernel, (sp_count, tp_count)), out_shape...]
    all_to_all x2 -> x0, starting transfers between devices: 12.9 us -> none  [the longest x1 7.36 us: shards(): lax.all_to_all(to_pieces(rotary, sp_count, tp_count), ('sp', 'tp'), split...]
    psum x1 -> x0, blocking collectives: 10.6 us -> none  [shards(): lax.psum(partial_value.astype(jnp.bfloat16), 'tp').astype(jnp.float32)]
    all_gather x2 -> x0, blocking collectives: 10.4 us -> none  [the longest x1 5.23 us: shards(): lax.all_gather(query_rotary, 'tp', axis=1, tiled=True)]
    unnamed x1 -> x0, blocking collectives: 5.76 us -> none
    all_to_all x2 -> x0, waiting for transfers between devices: 2.64 us -> none  [the longest x1 2.4 us: shards(): lax.all_to_all(to_pieces(hidden_summary, sp_count, tp_count), ('sp', 'tp'...]
    dot_general x7 -> x0, matrix products: 2.46 us -> none  [the longest x1 0.78 us: shards(): jnp.dot(flat_rows, narrowing_matrix, preferred_element_type=jnp.float32)]
    unnamed x22 -> x3, local copies, waits for them, and re-layouts: 2.26 us -> 4.58 us
  transfers between devices with their start and end apart: 2 -> 0, of which waited for: 2 -> 0; matrix products, arithmetic and copies ran while one was open for 7% -> 0% of each run, Pallas kernels for 0% -> 0%
where the time goes in v1:
time: 28.7 us; the launch traced here: 28.5 us
  Pallas kernels  22.3 us (78%)
  local copies, waits for them, and re-layouts  4.58 us (16%)
  other arithmetic  0.87 us (3%)
  between operations  0.66 us (2%)
    pallas_call x1, Pallas kernels, shards(): pl.pallas_call(functools.partial(kernel, (sp_count, tp_count)), out_shape...  22.3 us
    unnamed x3, local copies, waits for them, and re-layouts  4.58 us
    another operation x1, other arithmetic, shards(): table = jnp.stack([jnp.cos(angles), jnp.sin(angles)])  0.63 us

profile of v1, /device:TPU:0, one launch (start us, length us, event | category | flops | bytes accessed | tf_op | source)
XLA Modules:
  0.0 28.5 jit_solution(3390304148201006405)
XLA Ops:
  0.7 0.1 pad_maximum_fusion.1
  0.7 0.2 multiply_cosine_fusion
  0.9 0.6 %pad_maximum_fusion.table_ref = f32[2,40,64]{2,1,0:T(8,128)} fusion(f32[1,40,64]{2,1,0:T(8,128)S(1)} %get-tuple-element.13, f32[1,40,64]{2,1,0:T(8,128)S(1)} %get-tuple-element.12), kind=kLoop, calls=%fused_computation | loop fusion | flops 5120 | bytes 40960 | tf_op jit(solution)/shard_map/stack | solution.py:384
  1.5 22.3 %shard_map.112 = (bf16[32,32,128]{2,1,0:T(8,128)(2,1)}, bf16[1024,16]{1,0:T(8,128)(2,1)}, bf16[4,128]{1,0:T(4,128)(2,1)}) custom-call(bf16[8,32,2048]{2,1,0:T(8,128)(2,1)} %x_hbm.1, bf16[2048,512]{1,0:T(8,128)(2,1)} %w_hbm.1, bf16[64,2048]{1,0:T(8,128)(2,1)} %bitcast.8, bf16[128,16,128]{2,1,0:T(8,128)(2,1)} %lw_hbm.1, bf16[128,16,128]{2,1,0:T(8,128)(2,1)} %pw_hbm.1, ...), custom_call_target="tpu_custom_call" | custom-call | tf_op jit(solution)/shard_map/pallas_call | solution.py:388
  23.9 1.7 %copy.12 = bf16[1,1024,16]{1,2,0:T(8,128)(2,1)} copy(bf16[1,1024,16]{2,1,0:T(8,128)(2,1)} %bitcast.9) | data formatting | bytes 65536
  25.6 1.7 %copy.15 = bf16[1,1024,128]{2,1,0:T(8,128)(2,1)} copy(bf16[1,1024,128]{2,1,0:T(8,128)(2,1)} %bitcast.10) | data formatting | bytes 524288
  27.2 1.2 %copy.16 = bf16[1,4,128]{2,1,0:T(4,128)(2,1)} copy(bf16[1,4,128]{2,1,0:T(4,128)(2,1)} %bitcast.15) | data formatting | bytes 2048
  (2 shorter events, 0.0 us)

commit v2 on v1

--- a/solution.py
+++ b/solution.py
@@ -2,6 +2,7 @@
 
 import jax
 import jax.numpy as jnp
+import numpy as np
 from jax import lax
 from jax.experimental import pallas as pl
 from jax.experimental.pallas import tpu as pltpu
@@ -13,6 +14,7 @@
 norm_eps = 1e-06
 rotary_base = 10000.0
 LANES = 128
+VMEM_BYTES = 67043328
 ROW_CHUNKS = 2
 K_CHUNKS = 4
 MESH = pl.DeviceIdType.MESH
@@ -47,9 +49,9 @@
     wr_hbm,
     lw_hbm,
     pw_hbm,
+    table_hbm,
     gain_ref,
     sgain_ref,
-    table_ref,
     q_ref,
     qr_ref,
     cache_out,
@@ -72,9 +74,8 @@
     v_recv,
     spread,
     unpack,
-    rot_full,
+    table_ref,
     load_sem,
-    out_sem,
     lat_sem,
     rot_sem,
     q_send_sem,
@@ -108,8 +109,17 @@
         loads[key] = copy
 
     kdepth = features // K_CHUNKS
+    half_sp = sp_count // 2
+    my_half = lax.div(my_sp, half_sp)
+    in_half = lax.rem(my_sp, half_sp)
+
+    def target(order):
+        if order < half_sp:
+            return (1 - my_half) * half_sp + lax.rem(in_half + order, half_sp)
+        return my_half * half_sp + lax.rem(in_half + 1 + order - half_sp, half_sp)
+
     for j in range(seq_count):
-        load(("x", j), j, x_hbm.at[lax.rem(my_sp + 1 + j, sp_count)], x_ref.at[j])
+        load(("x", j), j, x_hbm.at[target(j)], x_ref.at[j])
     for k in range(K_CHUNKS):
         rows = pl.ds(k * kdepth, kdepth)
         load(("w", k), seq_count + k, w_hbm.at[rows], w_ref.at[rows])
@@ -117,6 +127,18 @@
     load("wr", base, wr_hbm, wr_ref)
     load("lw", base + 1, lw_hbm, lw_ref)
     load("pw", base + 2, pw_hbm, pw_ref)
+    load(
+        "table",
+        base + 3,
+        table_hbm.at[:, pl.ds(me * pos_local, pos_local)],
+        table_ref.at[:, pl.ds(0, pos_local)],
+    )
+    load(
+        "last",
+        base + 4,
+        table_hbm.at[:, pl.ds(total, 8)],
+        table_ref.at[:, pl.ds(pos_local, 8)],
+    )
 
     barrier = pltpu.get_barrier_semaphore()
 
@@ -136,8 +158,6 @@
     q_recv[my_tp, :, :plain] = q_ref[...].astype(f32)
     q_recv[my_tp, :, plain : plain + rope] = qr_ref[...].astype(f32)
 
-    cos = table_ref[0, :pos_local, :]
-    sin = table_ref[1, :pos_local, :]
     half = rope // 2
     row_r, col_r = iota((rope, rope), 0), iota((rope, rope), 1)
     swap = (
@@ -193,6 +213,10 @@
             acc = part if acc is None else acc + part
         if c == 0:
             loads["wr"].wait()
+            loads["table"].wait()
+            loads["last"].wait()
+        cos = table_ref[0, :pos_local, :]
+        sin = table_ref[1, :pos_local, :]
         rot = dot_t(xn_ref[...], wr_ref[...]).astype(bf16)
         hidden = rescaled_lines(acc.astype(bf16).astype(f32)) * sgain_ref[...]
         swapped = dot(rot, swap)
@@ -227,7 +251,7 @@
                 )
         for j in range(chunk_seq):
             order = c * chunk_seq + j
-            to_sp = lax.rem(my_sp + 1 + order, sp_count)
+            to_sp = target(order)
             for k in range(tp_count):
                 to_tp = lax.rem(my_tp + 1 + k, tp_count)
                 at = order * tp_count + to_tp
@@ -253,8 +277,8 @@
     )
     rkeep_shape = (total, LANES)
     rkeep = iota(rkeep_shape, 1) // rot_each == (iota(rkeep_shape, 0) % pos_local) // prow
-    narrow = (LANES, rot_each)
-    fold = one_hot(iota(narrow, 0) % rot_each == iota(narrow, 1))
+    narrow = (rot_each, LANES)
+    fold = one_hot(iota(narrow, 1) % rot_each == iota(narrow, 0))
 
     for copy in pairs:
         copy.wait()
@@ -278,17 +302,13 @@
     ).wait()
     rot_rows = rot_recv[...].astype(f32).reshape(n * prow, LANES).astype(bf16)
     rot_wide = jnp.where(rkeep, dot(unpack[...], rot_rows), 0.0).astype(bf16)
-    rot_cache = dot(rot_wide, fold).astype(bf16)
-    rot_full[...] = rot_cache
-    rot_store = pltpu.make_async_copy(rot_full, rotary_out, out_sem.at[1])
-    rot_store.start()
-    rot_part = dot_t(q_mine, rot_cache)
+    rot_cache = dot_t(fold, rot_wide).astype(bf16)
+    rotary_out[...] = rot_cache
+    rot_part = dot(q_mine, rot_cache)
 
     pltpu.make_async_copy(
         lat_recv.at[pl.ds(0, n - 1)], lat_recv.at[pl.ds(0, n - 1)], lat_sem.at[1]
     ).wait()
-    cache_store = pltpu.make_async_copy(lat_recv, cache_out, out_sem.at[0])
-    cache_store.start()
     cache = lat_recv[...].reshape(total, width)
     score_scale = (PLAIN_MATCH_SPAN + QK_ROPE) ** (-0.5)
     s_recv[my_tp] = ((dot_t(absorbed, cache) + rot_part) * score_scale).astype(bf16)
@@ -340,14 +360,35 @@
     pltpu.make_async_copy(
         stage.at[pl.ds(0, n - 1)], stage.at[pl.ds(0, n - 1)], lat_sem.at[0]
     ).wait()
-    cache_store.wait()
-    rot_store.wait()
+    cache_out[...] = lat_recv[...]
     for copy in pairs:
         copy.wait()
     summed = v_recv[0]
     for t in range(1, tp_count):
         summed = summed + v_recv[t]
     read_out[...] = rescaled_lines(summed).astype(bf16)
+
+
+def rotary_table(total, rope):
+    half = rope // 2
+    frequency = 1.0 / rotary_base ** (np.arange(half) * 2.0 / rope)
+    frequency = np.concatenate([frequency, frequency]).astype(np.float32)
+    spots = np.minimum(np.arange(total + 8), total).astype(np.float32)
+    angles = (spots[:, None] * frequency[None, :]).astype(np.float64)
+    return np.stack([np.cos(angles), np.sin(angles)]).astype(np.float32)
+
+
+def write_out(cache_ref, rotary_ref, read_ref, cache_hbm, rotary_hbm, read_hbm, sems):
+    copies = [
+        pltpu.make_async_copy(src, dst, sems.at[i])
+        for i, (src, dst) in enumerate(
+            ((cache_ref, cache_hbm), (rotary_ref, rotary_hbm), (read_ref, read_hbm))
+        )
+    ]
+    for copy in copies:
+        copy.start()
+    for copy in copies:
+        copy.wait()
 
 
 def shards(
@@ -374,26 +415,19 @@
     rot_each = rope // tp_count
     prow = pos_local * rot_each // LANES
     total = n * pos_local
-    block_index = lax.axis_index(("sp", "tp"))
-    half = rope // 2
-    frequency = 1.0 / rotary_base ** (jnp.arange(half, dtype=f32) * 2.0 / rope)
-    frequency = jnp.concatenate([frequency, frequency])
-    spots = jnp.arange(pos_local + 8, dtype=jnp.int32)
-    spots = jnp.where(spots < pos_local, block_index * pos_local + spots, total)
-    angles = spots.astype(f32)[:, None] * frequency[None, :]
-    table = jnp.stack([jnp.cos(angles), jnp.sin(angles)])
-    any_spec = pl.BlockSpec(memory_space=pl.ANY)
+    table = jnp.asarray(rotary_table(total, rope))
+    held = 2 * total * (max(width, LANES) + max(rot_each, 16)) + 52 * 1024
+    hbm_spec = pl.BlockSpec(memory_space=pltpu.HBM)
     vmem_spec = pl.BlockSpec(memory_space=pltpu.VMEM)
     dma = pltpu.SemaphoreType.DMA
     cache, rotary, read = pl.pallas_call(
         functools.partial(kernel, (sp_count, tp_count)),
         out_shape=(
-            jax.ShapeDtypeStruct((n, pos_local, width), bf16),
-            jax.ShapeDtypeStruct((total, rot_each), bf16),
-            jax.ShapeDtypeStruct((head_each, payload), bf16),
+            pltpu.VMEM((n, pos_local, width), bf16),
+            pltpu.VMEM((rot_each, total), bf16),
+            pltpu.VMEM((head_each, payload), bf16),
         ),
-        in_specs=[any_spec] * 5 + [vmem_spec] * 5,
-        out_specs=(any_spec, any_spec, vmem_spec),
+        in_specs=[hbm_spec] * 6 + [vmem_spec] * 4,
         scratch_shapes=[
             pltpu.VMEM((seq_count, pos_local, features), bf16),
             pltpu.VMEM((features, latent), bf16),
@@ -412,9 +446,8 @@
             pltpu.VMEM((tp_count, head_each, payload), f32),
             pltpu.VMEM((width * heads, width), bf16),
             pltpu.VMEM((total, n * prow), bf16),
-            pltpu.VMEM((total, rot_each), bf16),
-            dma((seq_count + K_CHUNKS + 3,)),
-            dma((2,)),
+            pltpu.VMEM((2, pos_local + 8, rope), f32),
+            dma((seq_count + K_CHUNKS + 5,)),
             dma((2,)),
             dma((2,)),
             dma((tp_count - 1,)),
@@ -425,7 +458,7 @@
             dma((tp_count - 1,)),
         ],
         compiler_params=pltpu.CompilerParams(
-            collective_id=0, has_side_effects=True, vmem_limit_bytes=63 * 1024 * 1024
+            collective_id=0, has_side_effects=True, vmem_limit_bytes=VMEM_BYTES - held
         ),
     )(
         layer_input,
@@ -433,15 +466,24 @@
         rotary_down.T,
         lookup_widening,
         payload_widening,
+        table,
         input_gain.reshape(1, -1),
         summary_scaling.reshape(1, -1),
-        table,
         query_nope[0],
         query_rotary[0],
     )
+    results = (cache, rotary, read)
+    cache, rotary, read = pl.pallas_call(
+        write_out,
+        out_shape=tuple(jax.ShapeDtypeStruct(r.shape, r.dtype) for r in results),
+        in_specs=[vmem_spec] * 3,
+        out_specs=(hbm_spec,) * 3,
+        scratch_shapes=[dma((3,))],
+        compiler_params=pltpu.CompilerParams(vmem_limit_bytes=1024 * 1024),
+    )(*results)
     return (
         cache.reshape(1, total, width),
-        rotary.reshape(1, total, rot_each),
+        rotary.T.reshape(1, total, rot_each),
         read.reshape(1, head_each, payload),
     )
 

time: 28.7 us -> 25.6 us (0.89)
  local copies, waits for them, and re-layouts: 4.58 us -> 0 us
  Pallas kernels: 22.3 us -> 24.7 us
  other arithmetic: 0.87 us -> 0 us
    unnamed x3 -> x0, local copies, waits for them, and re-layouts: 4.58 us -> none
    pallas_call x1, Pallas kernels: 22.3 us -> 24 us  [shards(): pl.pallas_call(functools.partial(kernel, (sp_count, tp_count)), out_shape...]
    pallas_call x0 -> x1, Pallas kernels: none -> 0.74 us  [shards(): pl.pallas_call(write_out, out_shape=tuple((jax.ShapeDtypeStruct(r.shape,...]
    another operation x1 -> x0, other arithmetic: 0.63 us -> none  [shards(): table = jnp.stack([jnp.cos(angles), jnp.sin(angles)])]
where the time goes in v2:
time: 25.6 us; the launch traced here: 25.4 us
  Pallas kernels  24.7 us (96%)
  between operations  0.64 us (2%)
    pallas_call x1, Pallas kernels, shards(): pl.pallas_call(functools.partial(kernel, (sp_count, tp_count)), out_shape...  24 us
    pallas_call x1, Pallas kernels, shards(): pl.pallas_call(write_out, out_shape=tuple((jax.ShapeDtypeStruct(r.shape,...  0.74 us

profile of v2, /device:TPU:0, one launch (start us, length us, event | category | flops | bytes accessed | tf_op | source)
XLA Modules:
  0.0 25.4 jit_solution(4329544915096172296)
XLA Ops:
  0.6 24.0 %shard_map.121 = (bf16[32,32,128]{2,1,0:T(8,128)(2,1)S(1)}, bf16[16,1024]{1,0:T(8,128)(2,1)S(1)}, bf16[4,128]{1,0:T(4,128)(2,1)S(1)}) custom-call(bf16[8,32,2048]{2,1,0:T(8,128)(2,1)} %x_hbm.1, bf16[2048,512]{1,0:T(8,128)(2,1)} %w_hbm.1, bf16[64,2048]{1,0:T(8,128)(2,1)} %bitcast.10, bf16[128,16,128]{2,1,0:T(8,128)(2,1)} %lw_hbm.1, ...), custom_call_target="tpu_custom_call" | custom-call | tf_op jit(solution)/shard_map/pallas_call | solution.py:423
  24.6 0.7 %shard_map.122 = (bf16[32,32,128]{2,1,0:T(8,128)(2,1)}, bf16[16,1024]{1,0:T(8,128)(2,1)}, bf16[4,128]{1,0:T(4,128)(2,1)}) custom-call(bf16[32,32,128]{2,1,0:T(8,128)(2,1)S(1)} %get-tuple-element.9.cache_ref, bf16[16,1024]{1,0:T(8,128)(2,1)S(1)} %get-tuple-element.10.rotary_ref, bf16[4,128]{1,0:T(4,128)(2,1)S(1)} %get-tuple-element.11.read_ref), custom_call_target="tpu_custom_call" | custom-call | tf_op jit(solution)/shard_map/pallas_call | solution.py:476

commit v3 on v2

--- a/solution.py
+++ b/solution.py
@@ -28,6 +28,18 @@
 
 def iota(shape, axis):
     return lax.broadcasted_iota(jnp.int32, shape, axis)
+
+
+def quot(values, by):
+    if by & (by - 1):
+        return values // by
+    return lax.shift_right_logical(values, jnp.int32(by.bit_length() - 1))
+
+
+def rest(values, by):
+    if by & (by - 1):
+        return values % by
+    return values & jnp.int32(by - 1)
 
 
 def one_hot(cond):
@@ -114,9 +126,7 @@
     in_half = lax.rem(my_sp, half_sp)
 
     def target(order):
-        if order < half_sp:
-            return (1 - my_half) * half_sp + lax.rem(in_half + order, half_sp)
-        return my_half * half_sp + lax.rem(in_half + 1 + order - half_sp, half_sp)
+        return lax.rem(my_sp + 1 + order, sp_count)
 
     for j in range(seq_count):
         load(("x", j), j, x_hbm.at[target(j)], x_ref.at[j])
@@ -167,7 +177,7 @@
     wide = (rope, tp_count * LANES)
     tile = one_hot(
         iota(wide, 0)
-        == iota(wide, 1) // LANES * rot_each + iota(wide, 1) % rot_each
+        == quot(iota(wide, 1), LANES) * rot_each + rest(iota(wide, 1), rot_each)
     )
 
     pairs = []
@@ -189,12 +199,13 @@
     pick_shape = (chunk_seq * prow, chunk)
     pick_row, pick_col = iota(pick_shape, 0), iota(pick_shape, 1)
     pick = one_hot(
-        (pick_row // prow == pick_col // pos_local) & (pick_row % prow == pick_col % prow)
+        (quot(pick_row, prow) == quot(pick_col, pos_local))
+        & (rest(pick_row, prow) == rest(pick_col, prow))
     )
     mask_shape = (chunk, tp_count * LANES)
-    keep = (iota(mask_shape, 1) % LANES) // rot_each == (
-        iota(mask_shape, 0) % pos_local
-    ) // prow
+    keep = quot(rest(iota(mask_shape, 1), LANES), rot_each) == quot(
+        rest(iota(mask_shape, 0), pos_local), prow
+    )
 
     for c in range(ROW_CHUNKS):
         for j in range(chunk_seq):
@@ -267,18 +278,21 @@
                     )
 
     spread_shape = spread.shape
-    spread[...] = one_hot(iota(spread_shape, 0) // heads == iota(spread_shape, 1))
+    spread[...] = one_hot(quot(iota(spread_shape, 0), heads) == iota(spread_shape, 1))
     own_shape = (heads, width * heads)
-    own_head = iota(own_shape, 0) == iota(own_shape, 1) % heads
+    own_head = iota(own_shape, 0) == rest(iota(own_shape, 1), heads)
     un_shape = unpack.shape
     un_row, un_col = iota(un_shape, 0), iota(un_shape, 1)
     unpack[...] = one_hot(
-        (un_row // pos_local == un_col // prow) & (un_row % prow == un_col % prow)
+        (quot(un_row, pos_local) == quot(un_col, prow))
+        & (rest(un_row, prow) == rest(un_col, prow))
     )
     rkeep_shape = (total, LANES)
-    rkeep = iota(rkeep_shape, 1) // rot_each == (iota(rkeep_shape, 0) % pos_local) // prow
+    rkeep = quot(iota(rkeep_shape, 1), rot_each) == quot(
+        rest(iota(rkeep_shape, 0), pos_local), prow
+    )
     narrow = (rot_each, LANES)
-    fold = one_hot(iota(narrow, 1) % rot_each == iota(narrow, 0))
+    fold = one_hot(rest(iota(narrow, 1), rot_each) == iota(narrow, 0))
 
     for copy in pairs:
         copy.wait()

time: 25.6 us -> 23.2 us (0.906)
  Pallas kernels: 24.7 us -> 22.4 us
    pallas_call x1, Pallas kernels: 24 us -> 21.7 us  [shards(): pl.pallas_call(functools.partial(kernel, (sp_count, tp_count)), out_shape...]
where the time goes in v3:
time: 23.2 us; the launch traced here: 23.1 us
  Pallas kernels  22.4 us (97%)
  between operations  0.64 us (3%)
    pallas_call x1, Pallas kernels, shards(): pl.pallas_call(functools.partial(kernel, (sp_count, tp_count)), out_shape...  21.7 us
    pallas_call x1, Pallas kernels, shards(): pl.pallas_call(write_out, out_shape=tuple((jax.ShapeDtypeStruct(r.shape,...  0.74 us

profile of v3, /device:TPU:0, one launch (start us, length us, event | category | flops | bytes accessed | tf_op | source)
XLA Modules:
  0.0 23.1 jit_solution(12497554302605127683)
XLA Ops:
  0.6 21.7 %shard_map.121 = (bf16[32,32,128]{2,1,0:T(8,128)(2,1)S(1)}, bf16[16,1024]{1,0:T(8,128)(2,1)S(1)}, bf16[4,128]{1,0:T(4,128)(2,1)S(1)}) custom-call(bf16[8,32,2048]{2,1,0:T(8,128)(2,1)} %x_hbm.1, bf16[2048,512]{1,0:T(8,128)(2,1)} %w_hbm.1, bf16[64,2048]{1,0:T(8,128)(2,1)} %bitcast.10, bf16[128,16,128]{2,1,0:T(8,128)(2,1)} %lw_hbm.1, ...), custom_call_target="tpu_custom_call" | custom-call | tf_op jit(solution)/shard_map/pallas_call | solution.py:437
  22.3 0.7 %shard_map.122 = (bf16[32,32,128]{2,1,0:T(8,128)(2,1)}, bf16[16,1024]{1,0:T(8,128)(2,1)}, bf16[4,128]{1,0:T(4,128)(2,1)}) custom-call(bf16[32,32,128]{2,1,0:T(8,128)(2,1)S(1)} %get-tuple-element.9.cache_ref, bf16[16,1024]{1,0:T(8,128)(2,1)S(1)} %get-tuple-element.10.rotary_ref, bf16[4,128]{1,0:T(4,128)(2,1)S(1)} %get-tuple-element.11.read_ref), custom_call_target="tpu_custom_call" | custom-call | tf_op jit(solution)/shard_map/pallas_call | solution.py:490

commit v4 on v3

--- a/solution.py
+++ b/solution.py
@@ -264,7 +264,7 @@
             order = c * chunk_seq + j
             to_sp = target(order)
             for k in range(tp_count):
-                to_tp = lax.rem(my_tp + 1 + k, tp_count)
+                to_tp = lax.rem(my_tp + tp_count - 1 - k, tp_count)
                 at = order * tp_count + to_tp
                 if order == seq_count - 1 and k == tp_count - 1:
                     lat_recv[me] = stage[at]

time: 23.2 us -> 22.9 us (0.987)
  Pallas kernels: 22.4 us -> 22.1 us
    pallas_call x1, Pallas kernels: 21.7 us -> 21.4 us  [shards(): pl.pallas_call(functools.partial(kernel, (sp_count, tp_count)), out_shape...]
where the time goes in v4:
time: 22.9 us; the launch traced here: 22.8 us
  Pallas kernels  22.1 us (97%)
  between operations  0.64 us (3%)
    pallas_call x1, Pallas kernels, shards(): pl.pallas_call(functools.partial(kernel, (sp_count, tp_count)), out_shape...  21.4 us
    pallas_call x1, Pallas kernels, shards(): pl.pallas_call(write_out, out_shape=tuple((jax.ShapeDtypeStruct(r.shape,...  0.74 us

profile of v4, /device:TPU:0, one launch (start us, length us, event | category | flops | bytes accessed | tf_op | source)
XLA Modules:
  0.0 22.8 jit_solution(17060359612334335585)
XLA Ops:
  0.6 21.4 %shard_map.121 = (bf16[32,32,128]{2,1,0:T(8,128)(2,1)S(1)}, bf16[16,1024]{1,0:T(8,128)(2,1)S(1)}, bf16[4,128]{1,0:T(4,128)(2,1)S(1)}) custom-call(bf16[8,32,2048]{2,1,0:T(8,128)(2,1)} %x_hbm.1, bf16[2048,512]{1,0:T(8,128)(2,1)} %w_hbm.1, bf16[64,2048]{1,0:T(8,128)(2,1)} %bitcast.10, bf16[128,16,128]{2,1,0:T(8,128)(2,1)} %lw_hbm.1, ...), custom_call_target="tpu_custom_call" | custom-call | tf_op jit(solution)/shard_map/pallas_call | solution.py:437
  22.0 0.7 %shard_map.122 = (bf16[32,32,128]{2,1,0:T(8,128)(2,1)}, bf16[16,1024]{1,0:T(8,128)(2,1)}, bf16[4,128]{1,0:T(4,128)(2,1)}) custom-call(bf16[32,32,128]{2,1,0:T(8,128)(2,1)S(1)} %get-tuple-element.9.cache_ref, bf16[16,1024]{1,0:T(8,128)(2,1)S(1)} %get-tuple-element.10.rotary_ref, bf16[4,128]{1,0:T(4,128)(2,1)S(1)} %get-tuple-element.11.read_ref), custom_call_target="tpu_custom_call" | custom-call | tf_op jit(solution)/shard_map/pallas_call | solution.py:490
